TPU v7x, 32 devices: a whole 2x2x4 slice. The times are simulated.
32 devices in a mesh: fs: 4 (over y, x), tp: 8 (over z, core).
Axes of the slice: x: 2, y: 2, z: 4, core: 2. Of those that a mesh axis runs over, the one named last changes fastest.
Arguments:
- tokens: bfloat16 [2048, 2048], P('fs', 'tp'), may hold values from -6 to 6
- norm_gain: float32 [2048], P('fs'), may hold values from 0.1 to 1.9
- gate_train: float32 [2048, 8192], P('fs', 'tp'), may hold values from -0.125 to 0.125
- up_train: float32 [2048, 8192], P('fs', 'tp'), may hold values from -0.125 to 0.125
- down_train: float32 [8192, 2048], P('fs', 'tp'), may hold values from -0.0625 to 0.0625
Outputs:
- gate_serve: bfloat16 [2048, 8192], P(None, 'tp')
- up_serve: bfloat16 [2048, 8192], P(None, 'tp')
- down_serve: bfloat16 [8192, 2048], P('tp')
- layer_out: bfloat16 [2048, 2048], P(('fs', 'tp'))
All inputs are finite; a program needn't handle non-finite values.
Results may differ from a plain program's by a relative error of at most 0.024.
Values may be sent and summed in bfloat16 or wider, within the bound.
A program may use at most 64 MiB of HBM per device.

v0:
```python
import functools

import jax
import jax.numpy as jnp
from jax import lax
from jax.experimental import pallas as pl
from jax.experimental.pallas import tpu as pltpu
from jax.sharding import PartitionSpec as P

MESH = pl.DeviceIdType.MESH
BF16 = jnp.bfloat16
F32 = jnp.float32
epsilon = 1e-06
CHUNKS = 4
X_ORDER = (0, 1, 2, 3)
Y_ORDER = (2, 3, 0, 1)
QUARTERS = 4
LAG = 2


def flip(a, k):
    result = 0
    for bit in (1, 2, 4):
        own, other = (a // bit) % 2, (k // bit) % 2
        result = result + bit * (own + other - 2 * own * other)
    return result


def kernel(
    tok_in, gain_in, gate_in, up_in, down_in,
    wbuf, dbuf, layer_out,
    w32, d32, dcast, tbuf, acc, hidden, scale, keep, psend, precv, zsend, zrecv,
    load_w, load_d, tok_s, tok_r, own_s, fwd_s, w_r, dz_s, d_s, d_r, p_s, p_r, z_s, z_r,
):
    f, t = lax.axis_index("fs"), lax.axis_index("tp")
    n_tp, n_fs = tbuf.shape[0], wbuf.shape[1]
    z, core = t // 2, t % 2
    fx, fy, fd = flip(f, 1), flip(f, 2), flip(f, 3)
    mate = flip(t, 1)
    rows = wbuf.shape[2]
    part = rows // CHUNKS
    w_ins = (gate_in, up_in)
    tall, width = dbuf.shape[1], dbuf.shape[2]
    quarter = tall // QUARTERS
    per = n_tp // n_fs
    n_tok = tbuf.shape[1]
    piece_rows = n_tok // n_tp

    def remote(src, dst, ss, rs, to_f, to_t):
        return pltpu.make_async_remote_copy(
            src_ref=src, dst_ref=dst, send_sem=ss, recv_sem=rs, device_id=(to_f, to_t), device_id_type=MESH
        )

    def load(w, i):
        return pltpu.make_async_copy(w_ins[w].at[pl.ds(i * part, part)], w32.at[w, pl.ds(i * part, part)], load_w.at[w, i])

    order = (0, 2, 1, 3)
    for i in order:
        for w in range(2):
            load(w, i).start()
    load_down = [
        pltpu.make_async_copy(down_in.at[pl.ds(c * tall, tall)], d32.at[pl.ds(c * tall, tall)], load_d.at[c])
        for c in range(per)
    ]
    for copy in load_down:
        copy.start()

    barrier = pltpu.get_barrier_semaphore()
    peers = [(fx, t), (fy, t)] + [(f, flip(t, k)) for k in range(1, n_tp)]
    for peer in peers:
        pl.semaphore_signal(barrier, inc=1, device_id=peer, device_id_type=MESH)

    tbuf[t] = tok_in[...]

    def cast(w, i):
        block = pl.ds(i * part, part)
        load(w, i).wait()
        wbuf[w, f, block] = (gain_in[block] * w32[w, block]).astype(BF16)

    pl.semaphore_wait(barrier, len(peers))

    def tok_copy(src, piece, slot, to):
        return remote(src, tbuf.at[piece], tok_s.at[slot], tok_r.at[piece], f, to)

    for slot, k in enumerate((1, 2, 4, 6)):
        tok_copy(tok_in, t, slot, flip(t, k)).start()

    def w_copy(w, src, i, sem, to):
        ref = wbuf.at[w, src, pl.ds(i * part, part)]
        return remote(ref, ref, sem, w_r.at[w, src, i], to, t)

    def send_own(step, w):
        w_copy(w, f, X_ORDER[step], own_s.at[0, w, X_ORDER[step]], fx).start()
        w_copy(w, f, Y_ORDER[step], own_s.at[1, w, Y_ORDER[step]], fy).start()

    waiting = None
    for step in range(CHUNKS // 2):
        for w in range(2):
            cast(w, X_ORDER[step])
            cast(w, Y_ORDER[step])
            if waiting is not None:
                send_own(*waiting)
            waiting = (step, w)

    def dz_copy(c, h):
        block = pl.ds(h * quarter, quarter)
        return remote(dcast.at[c, block], dbuf.at[t, block], dz_s.at[c, h], d_r.at[t, h], f, f * per + c)

    for c in range(per):
        load_down[c].wait()
        for h in range(QUARTERS):
            block = pl.ds(h * quarter, quarter)
            dcast[c, block] = d32[pl.ds(c * tall + h * quarter, quarter)].astype(BF16)

        @pl.when(t == f * per + c)
        def _():
            dbuf[t] = dcast[c]

        if c == 0:
            send_own(*waiting)
            for step in range(CHUNKS // 2, CHUNKS):
                for w in range(2):
                    send_own(step, w)

    for h in range(QUARTERS):
        for c in range(per):
            @pl.when(t != f * per + c)
            def _():
                dz_copy(c, h).start()

    def arrive(step, w):
        i = X_ORDER[step]
        w_copy(w, fx, i, fwd_s.at[w, i], fy).wait_recv()
        if i < CHUNKS // 2:
            w_copy(w, fx, i, fwd_s.at[w, i], fy).start()
        i = Y_ORDER[step]
        w_copy(w, fy, i, fwd_s.at[w, i], fx).wait_recv()
        if i >= CHUNKS // 2:
            w_copy(w, fy, i, fwd_s.at[w, i], fx).start()

    tile = 512

    def accumulate(src, first):
        def one(n, _):
            w, column = n // (wbuf.shape[3] // tile), pl.multiple_of(n % (wbuf.shape[3] // tile) * tile, tile)
            total = 0.0 if first else acc[w, :, pl.ds(column, tile)]
            for p in range(per):
                total = total + jnp.dot(
                    tbuf[src * per + p],
                    wbuf[w, src, pl.ds(p * width, width), pl.ds(column, tile)],
                    preferred_element_type=F32,
                )
            acc[w, :, pl.ds(column, tile)] = total
            return 0

        lax.fori_loop(0, 2 * (wbuf.shape[3] // tile), one, 0)

    for step in range(CHUNKS // 2):
        for w in range(2):
            arrive(step, w)
    for slot, k in enumerate((2, 4, 6)):
        piece = flip(t, k)
        tok_copy(tok_in, piece, 4 + slot, mate).wait_recv()
        tok_copy(tbuf.at[piece], piece, 4 + slot, mate).start()
    for k in (1, 3, 5, 7):
        tok_copy(tok_in, flip(t, k), 0, mate).wait_recv()
    step_rows = n_tok // n_tp

    def norm(i, _):
        block = pl.ds(i * step_rows, step_rows)
        squares = 0.0
        for p in range(n_tp):
            wide = tbuf[p, block].astype(F32)
            squares = squares + wide * wide
        scale[block] = lax.rsqrt(jnp.sum(squares, axis=1, keepdims=True) / (n_tp * width) + epsilon)
        return 0

    lax.fori_loop(0, n_tp, norm, 0)
    accumulate(f, True)
    for step in range(CHUNKS // 2, CHUNKS):
        for w in range(2):
            arrive(step, w)

    owner = t // per
    low, high = (f % 2 + owner % 2) % 2, (f // 2 + owner // 2) % 2
    is_source = f == owner
    to_first = fx + (fy - fx) * (low * (1 - high))
    to_second = fy + (fx - fy) * ((1 - low) * high)
    ends = ((1 - low) * high, low * (1 - high))
    nexts = (to_first, to_second)

    def d_copy(piece, h):
        ref = dbuf.at[piece, pl.ds(h * quarter, quarter)]
        return remote(ref, ref, d_s.at[piece, h], d_r.at[piece, h], nexts[h % 2], t)

    def pass_on(k):
        piece = flip(t, k)
        for h in range(QUARTERS):
            @pl.when(ends[h % 2] == 0)
            def _():
                if isinstance(k, int) and k == 0:
                    @pl.when(jnp.logical_not(is_source))
                    def _():
                        d_copy(piece, h).wait_recv()
                else:
                    d_copy(piece, h).wait_recv()
                d_copy(piece, h).start()

    def take_last(k):
        piece = flip(t, k)
        for h in range(QUARTERS):
            @pl.when(ends[h % 2] == 1)
            def _():
                d_copy(piece, h).wait_recv()

    @pl.when(is_source)
    def _():
        pass_on(0)
        pass_on(1)

    accumulate(fx, False)
    accumulate(fy, False)
    for i in (0, 2, 1, 3):
        for w in range(2):
            w_copy(w, fd, i, fwd_s.at[w, i], fx).wait_recv()
    accumulate(fd, False)

    @pl.when(jnp.logical_not(is_source))
    def _():
        pass_on(0)

    def make_hidden(n, _):
        columns = pl.ds(pl.multiple_of(n * tile, tile), tile)
        s = scale[...]
        g = acc[0, :, columns] * s
        hidden[:, columns] = (g / (1.0 + jnp.exp(-g)) * (acc[1, :, columns] * s)).astype(BF16)
        return 0

    lax.fori_loop(0, hidden.shape[1] // tile, make_hidden, 0)

    def p_copy(k):
        return remote(psend.at[k], precv.at[k], p_s.at[k], p_r.at[k], f, mate)

    def z_copy(k, dz, piece):
        to = flip(t, 2 * dz)
        return remote(zsend.at[k, to // 2], zrecv.at[z, piece], z_s.at[k, dz], z_r.at[z, piece], f, to)

    def z_arrival(dz, piece):
        src = flip(t, 2 * dz)
        return remote(zsend.at[0, 0], zrecv.at[src // 2, piece], z_s.at[0, dz], z_r.at[src // 2, piece], f, src)

    n_z = n_tp // 2

    def finish(k):
        p_copy(k).wait_recv()
        for b in range(n_z):
            block = (keep[flip(k, 1), b] + precv[k, b].astype(F32)).astype(BF16)
            zsend[k, b] = block
        piece = flip(mate, k)
        zrecv[z, piece] = zsend[k, z]
        for dz in range(1, n_z):
            z_copy(k, dz, piece).start()

    def product(k):
        piece = flip(t, k)
        out = jnp.dot(hidden[...], dbuf[piece], preferred_element_type=F32)
        out = out.reshape(n_z, 2, piece_rows, width)

        @pl.when(core == 0)
        def _():
            keep[k] = out[:, 0]
            psend[k] = out[:, 1].astype(BF16)

        @pl.when(core == 1)
        def _():
            keep[k] = out[:, 1]
            psend[k] = out[:, 0].astype(BF16)

        p_copy(k).start()

    @pl.when(jnp.logical_not(is_source))
    def _():
        pass_on(1)

    def step(i, _):
        made, done = i, i - 2

        @pl.when(i + LAG < n_tp)
        def _():
            pass_on(i + LAG)

        @pl.when(made < n_tp)
        def _():
            take_last(made)
            product(made)

        @pl.when(done >= 0)
        def _():
            finish(done)

        return 0

    lax.fori_loop(0, n_tp + 2, step, 0)

    for k in range(n_tp):
        for dz in range(1, n_z):
            z_arrival(dz, k).wait_recv()
    for piece in range(n_tp):
        total = zrecv[0, piece].astype(F32)
        for b in range(1, n_z):
            total = total + zrecv[b, piece].astype(F32)
        layer_out[:, pl.ds(piece * width, width)] = total.astype(BF16)

    for slot in range(4):
        tok_copy(tok_in, t, slot, mate).wait_send()
    for slot in range(3):
        tok_copy(tok_in, t, 4 + slot, mate).wait_send()
    for w in range(2):
        for i in range(CHUNKS):
            w_copy(w, f, i, own_s.at[0, w, i], fx).wait_send()
            w_copy(w, f, i, own_s.at[1, w, i], fy).wait_send()
            w_copy(w, f, i, fwd_s.at[w, i], fx).wait_send()
    for c in range(per):
        for h in range(QUARTERS):
            @pl.when(t != f * per + c)
            def _():
                dz_copy(c, h).wait_send()
    for k in range(n_tp):
        p_copy(k).wait_send()
        for dz in range(1, n_z):
            z_copy(k, dz, k).wait_send()
        for h in range(QUARTERS):
            @pl.when(ends[h % 2] == 0)
            def _():
                d_copy(k, h).wait_send()


def write_out(weights, down, layer, gate_out, up_out, down_out, layer_out, w_s, d_s, l_s):
    _, n_fs, rows, _ = weights.shape
    n_tp, _, width = down.shape
    copies = [pltpu.make_async_copy(layer, layer_out, l_s)]
    for w, out in enumerate((gate_out, up_out)):
        for src in range(n_fs):
            copies.append(pltpu.make_async_copy(weights.at[w, src], out.at[pl.ds(src * rows, rows)], w_s.at[w, src]))
    for j in range(n_tp):
        copies.append(pltpu.make_async_copy(down.at[j], down_out.at[:, pl.ds(j * width, width)], d_s.at[j]))
    for copy in copies:
        copy.start()
    for copy in copies:
        copy.wait()


def body(tokens, norm_gain, gate_train, up_train, down_train, *, n_fs, n_tp):
    n_tok, width = tokens.shape
    rows, cols = gate_train.shape
    tall = down_train.shape[0] * n_fs // n_tp
    piece_rows = n_tok // n_tp
    n_z = n_tp // 2
    hbm = pl.BlockSpec(memory_space=pl.ANY)
    vmem = pl.BlockSpec(memory_space=pltpu.VMEM)
    dma = pltpu.SemaphoreType.DMA
    weights, down, layer = pl.pallas_call(
        kernel,
        out_shape=(
            pltpu.VMEM((2, n_fs, rows, cols), BF16),
            pltpu.VMEM((n_tp, tall, width), BF16),
            pltpu.VMEM((piece_rows, width * n_tp), BF16),
        ),
        in_specs=[vmem, vmem, hbm, hbm, hbm],
        out_specs=(vmem, vmem, vmem),
        scratch_shapes=[
            pltpu.VMEM((2, rows, cols), F32),
            pltpu.VMEM(down_train.shape, F32),
            pltpu.VMEM((n_tp // n_fs, tall, width), BF16),
            pltpu.VMEM((n_tp, n_tok, width), BF16),
            pltpu.VMEM((2, n_tok, cols), F32),
            pltpu.VMEM((n_tok, cols), BF16),
            pltpu.VMEM((n_tok, 1), F32),
            pltpu.VMEM((n_tp, n_z, piece_rows, width), F32),
            pltpu.VMEM((n_tp, n_z, piece_rows, width), BF16),
            pltpu.VMEM((n_tp, n_z, piece_rows, width), BF16),
            pltpu.VMEM((n_tp, n_z, piece_rows, width), BF16),
            pltpu.VMEM((n_z, n_tp, piece_rows, width), BF16),
            dma((2, CHUNKS)),
            dma((n_tp // n_fs,)),
            dma((7,)),
            dma((n_tp,)),
            dma((2, 2, CHUNKS)),
            dma((2, CHUNKS)),
            dma((2, n_fs, CHUNKS)),
            dma((n_tp // n_fs, QUARTERS)),
            dma((n_tp, QUARTERS)),
            dma((n_tp, QUARTERS)),
            dma((n_tp,)),
            dma((n_tp,)),
            dma((n_tp, n_z)),
            dma((n_z, n_tp)),
        ],
        compiler_params=pltpu.CompilerParams(
            collective_id=0, has_side_effects=True, vmem_limit_bytes=36 * 1024 * 1024
        ),
    )(tokens, norm_gain[:, None], gate_train, up_train, down_train)
    return pl.pallas_call(
        write_out,
        out_shape=(
            jax.ShapeDtypeStruct((rows * n_fs, cols), BF16),
            jax.ShapeDtypeStruct((rows * n_fs, cols), BF16),
            jax.ShapeDtypeStruct((tall, width * n_tp), BF16),
            jax.ShapeDtypeStruct((piece_rows, width * n_tp), BF16),
        ),
        in_specs=[vmem] * 3,
        out_specs=(hbm,) * 4,
        scratch_shapes=[dma((2, n_fs)), dma((n_tp,)), dma],
        compiler_params=pltpu.CompilerParams(vmem_limit_bytes=4 * 1024 * 1024),
    )(weights, down, layer)


def plain(tokens, norm_gain, gate_train, up_train, down_train):
    gate_local = (norm_gain[:, None] * gate_train).astype(BF16)
    up_local = (norm_gain[:, None] * up_train).astype(BF16)
    down_local = down_train.astype(BF16)
    features = lax.all_gather(tokens, "tp", axis=1, tiled=True)
    wide = features.astype(F32)
    squares = jnp.sum(wide * wide, axis=1)
    gate_whole = lax.all_gather(gate_local, "fs", axis=0, tiled=True)
    up_whole = lax.all_gather(up_local, "fs", axis=0, tiled=True)
    gate_sum = jnp.dot(features, gate_whole, preferred_element_type=F32)
    up_sum = jnp.dot(features, up_whole, preferred_element_type=F32)
    down_rows = lax.all_gather(down_local, "fs", axis=0, tiled=True)
    down_whole = lax.all_to_all(down_rows, "tp", split_axis=0, concat_axis=1, tiled=True)
    scale = lax.rsqrt(squares / features.shape[1] + epsilon)[:, None]
    hidden = (jax.nn.silu(gate_sum * scale) * (up_sum * scale)).astype(BF16)
    mixed = lax.psum_scatter(
        jnp.dot(hidden, down_whole, preferred_element_type=F32).astype(BF16), "tp", scatter_dimension=0, tiled=True
    )
    return (gate_whole, up_whole, down_whole, mixed)


def solution(mesh):
    n_fs, n_tp = mesh.shape["fs"], mesh.shape["tp"]
    fast = n_fs == 4 and n_tp == 8
    return jax.shard_map(
        functools.partial(body, n_fs=n_fs, n_tp=n_tp) if fast else plain,
        mesh=mesh,
        in_specs=(P("fs", "tp"), P("fs"), P("fs", "tp"), P("fs", "tp"), P("fs", "tp")),
        out_specs=(P(None, "tp"), P(None, "tp"), P("tp", None), P(("fs", "tp"), None)),
        check_vma=False,
    )
```

profile of v0, /device:TPU:0, one launch (start us, length us, event | category | flops | bytes accessed | tf_op | source)
XLA Modules:
  0.0 154.0 jit_solution(17520797859831466538)
XLA Ops:
  0.6 0.8 copy.9.gain_in
  1.5 0.0 copy-start
  1.5 1.6 %copy-done = f32[512,1024]{1,0:T(8,128)S(1)} copy-done((f32[512,1024]{1,0:T(8,128)S(1)}, f32[512,1024]{1,0:T(8,128)}, u32[]{:S(2)}) %copy-start) | copy-done | bytes 2097176
  3.1 0.0 copy-start.1
  3.1 1.6 %copy-done.1 = f32[512,1024]{1,0:T(8,128)S(1)} copy-done((f32[512,1024]{1,0:T(8,128)S(1)}, f32[512,1024]{1,0:T(8,128)}, u32[]{:S(2)}) %copy-start.1) | copy-done | bytes 2097176
  4.6 0.0 copy-start.2
  4.6 0.9 copy-done.2
  5.6 143.7 %shard_map.84 = (bf16[2,4,512,1024]{3,2,1,0:T(8,128)(2,1)S(1)}, bf16[8,1024,256]{2,1,0:T(8,128)(2,1)S(1)}, bf16[64,2048]{1,0:T(8,128)(2,1)S(1)}) custom-call(bf16[512,256]{1,0:T(8,128)(2,1)S(1)} %copy-done.2, f32[512,1]{1,0:T(8,128)S(1)} %copy.9.gain_in, f32[512,1024]{1,0:T(8,128)S(1)} %copy-done, f32[512,1024]{1,0:T(8,128)S(1)} %copy-done.1, ...), custom_call_target="tpu_custom_call" | custom-call | tf_op jit(solution)/shard_map/pallas_call | solution.py:362
  149.3 4.8 %shard_map.85 = (bf16[2048,1024]{1,0:T(8,128)(2,1)}, bf16[2048,1024]{1,0:T(8,128)(2,1)}, bf16[1024,2048]{1,0:T(8,128)(2,1)}, bf16[64,2048]{1,0:T(8,128)(2,1)}) custom-call(bf16[2,4,512,1024]{3,2,1,0:T(8,128)(2,1)S(1)} %get-tuple-element.7.weights, bf16[8,1024,256]{2,1,0:T(8,128)(2,1)S(1)} %get-tuple-element.8.down, bf16[64,2048]{1,0:T(8,128)(2,1)S(1)} %get-tuple-element.9.layer), custom_call_target="tpu_custom_call" | custom-call | tf_op jit(solution)/shard_map/pallas_call | solution.py:403
Async XLA Ops:
  1.5 1.6 %copy-start = (f32[512,1024]{1,0:T(8,128)S(1)}, f32[512,1024]{1,0:T(8,128)}, u32[]{:S(2)}) copy-start(f32[512,1024]{1,0:T(8,128)} %gate_in.1) | copy-start | bytes 6291460
  3.1 1.6 %copy-start.1 = (f32[512,1024]{1,0:T(8,128)S(1)}, f32[512,1024]{1,0:T(8,128)}, u32[]{:S(2)}) copy-start(f32[512,1024]{1,0:T(8,128)} %up_in.1) | copy-start | bytes 6291460
  4.6 0.9 copy-start.2
where the time goes:
time: 154 us
  Pallas kernels  148 us (96%)
  local copies, waits for them, and re-layouts  4.95 us (3%)
    pallas_call x1, Pallas kernels, body(): pl.pallas_call(kernel, out_shape=(pltpu.VMEM((2, n_fs, rows, cols), BF16)...  144 us
    pallas_call x1, Pallas kernels, body(): pl.pallas_call(write_out, out_shape=(jax.ShapeDtypeStruct((rows * n_fs, c...  4.77 us
    unnamed x6, local copies, waits for them, and re-layouts  4.13 us

commit v1 on v0

v1 whole, which is shorter than its diff:
```python
import functools

import jax
import jax.numpy as jnp
from jax import lax
from jax.experimental import pallas as pl
from jax.experimental.pallas import tpu as pltpu
from jax.sharding import PartitionSpec as P

MESH = pl.DeviceIdType.MESH
BF16 = jnp.bfloat16
F32 = jnp.float32
epsilon = 1e-06
CHUNKS = 4
X_ORDER = (0, 1, 2, 3)
Y_ORDER = (2, 3, 0, 1)
QUARTERS = 4
DUAL = (0, 1)
CHAIN = (2, 3)
scope = jax.named_scope


def flip(a, k):
    result = 0
    for bit in (1, 2, 4):
        own, other = (a // bit) % 2, (k // bit) % 2
        result = result + bit * (own + other - 2 * own * other)
    return result


def kernel(
    tok_in, gain_in, gate_in, up_in, down_in,
    wbuf, dbuf, layer_out,
    gain, w32, d32, dcast, xbuf, tbuf, acc, hidden, scale, keep, psend, precv, zsend, zrecv,
    load_g, load_t, load_w, load_d, tok_s, tok_r, own_s, fwd_s, w_r, dz_s, o_s, o_r, zr_s, d_s, d_r, p_s, p_r, z_s, z_r,
):
    f, t = lax.axis_index("fs"), lax.axis_index("tp")
    n_tp, n_fs = tbuf.shape[0], wbuf.shape[1]
    z, core = t // 2, t % 2
    fx, fy, fd = flip(f, 1), flip(f, 2), flip(f, 3)
    mate = flip(t, 1)
    rows = wbuf.shape[2]
    part = rows // CHUNKS
    w_ins = (gate_in, up_in)
    tall, width = dbuf.shape[1], dbuf.shape[2]
    quarter = tall // QUARTERS
    per = n_tp // n_fs
    n_tok = tbuf.shape[1]
    piece_rows = n_tok // n_tp
    n_z = n_tp // 2
    q = flip(f, z)
    side = jnp.logical_or(q == 1, q == 2)
    toward = fx + (fy - fx) * (q // 2)
    away = fy + (fx - fy) * (q // 2)

    def remote(src, dst, ss, rs, to_f, to_t):
        return pltpu.make_async_remote_copy(
            src_ref=src, dst_ref=dst, send_sem=ss, recv_sem=rs, device_id=(to_f, to_t), device_id_type=MESH
        )

    def load(w, i):
        return pltpu.make_async_copy(w_ins[w].at[pl.ds(i * part, part)], w32.at[w, pl.ds(i * part, part)], load_w.at[w, i])

    barrier = pltpu.get_barrier_semaphore()
    peers = [(fx, t), (fy, t)] + [(f, flip(t, k)) for k in range(1, n_tp)]
    for peer in peers:
        pl.semaphore_signal(barrier, inc=1, device_id=peer, device_id_type=MESH)

    load_gain = pltpu.make_async_copy(gain_in, gain, load_g)
    load_tok = pltpu.make_async_copy(tok_in, tbuf.at[t], load_t)
    load_down = [
        pltpu.make_async_copy(down_in.at[pl.ds(c * tall, tall)], d32.at[pl.ds(c * tall, tall)], load_d.at[c])
        for c in range(per)
    ]
    load_gain.start()
    for i in (0, 2):
        for w in range(2):
            load(w, i).start()
    load_tok.start()
    for copy in load_down:
        copy.start()
    for i in (1, 3):
        for w in range(2):
            load(w, i).start()

    def cast(w, i):
        block = pl.ds(i * part, part)
        load(w, i).wait()
        lanes = 128
        tall_gain = jnp.broadcast_to(gain[:, block], (lanes, part)).T
        for j in range(wbuf.shape[3] // lanes):
            columns = pl.ds(j * lanes, lanes)
            wbuf[w, f, block, columns] = (tall_gain * w32[w, block, columns]).astype(BF16)

    def tok_copy(src, piece, slot, to):
        return remote(src, tbuf.at[piece], tok_s.at[slot], tok_r.at[piece], f, to)

    def w_copy(w, src, i, sem, to):
        ref = wbuf.at[w, src, pl.ds(i * part, part)]
        return remote(ref, ref, sem, w_r.at[w, src, i], to, t)

    def send_own(step, w):
        w_copy(w, f, X_ORDER[step], own_s.at[0, w, X_ORDER[step]], fx).start()
        w_copy(w, f, Y_ORDER[step], own_s.at[1, w, Y_ORDER[step]], fy).start()

    def rows_of(h):
        return pl.ds(h * quarter, quarter)

    def dz_copy(c, h):
        return remote(dcast.at[c, rows_of(h)], dbuf.at[t, rows_of(h)], dz_s.at[c, h], d_r.at[t, h], f, f * per + c)

    def o_copy(slot, c, h, to):
        return remote(dcast.at[c, rows_of(h)], xbuf.at[slot, c, rows_of(h)], o_s.at[0, c, h], o_r.at[slot, c, h], to, t)

    def transit(c, h, to):
        ref = xbuf.at[2, c, rows_of(h)]
        return remote(ref, ref, o_s.at[1, c, h], o_r.at[2, c, h], to, t)

    def over_z(slot, c, h, column):
        return remote(
            xbuf.at[slot, c, rows_of(h)], dbuf.at[t, rows_of(h)], zr_s.at[slot, c, h], d_r.at[t, h], f, column * per + c
        )

    def d_copy(piece, h, to):
        ref = dbuf.at[piece, rows_of(h)]
        return remote(ref, ref, d_s.at[piece, h], d_r.at[piece, h], to, t)

    chain_stops = (q == 2, q == 1)
    chain_to = (fx + (fy - fx) * (q % 2) * (1 - q // 2), fy + (fx - fy) * (1 - q % 2) * (q // 2))

    def chain(k, h):
        piece = flip(t, k)

        @pl.when(jnp.logical_not(chain_stops[h % 2]))
        def _():
            if isinstance(k, int) and k == 0:
                @pl.when(q != 0)
                def _():
                    d_copy(piece, h, chain_to[h % 2]).wait_recv()
            else:
                d_copy(piece, h, chain_to[h % 2]).wait_recv()
            d_copy(piece, h, chain_to[h % 2]).start()

    def own_chain():
        for k in range(per):
            for h in range(QUARTERS):
                chain(k, h)

    def hand(k, h, to):
        piece = flip(t, k)
        d_copy(piece, h, to).wait_recv()
        d_copy(piece, h, to).start()

    load_gain.wait()
    cast(0, X_ORDER[0])
    cast(0, Y_ORDER[0])
    with scope("barrier"):
        pl.semaphore_wait(barrier, len(peers))
    cast(1, X_ORDER[0])
    cast(1, Y_ORDER[0])
    send_own(0, 0)
    load_tok.wait()
    for slot, k in enumerate((1, 2, 4, 6)):
        tok_copy(tbuf.at[t], t, slot, flip(t, k)).start()

    for c in range(per):
        load_down[c].wait()
        for h in range(QUARTERS):
            dcast[c, rows_of(h)] = d32[pl.ds(c * tall + h * quarter, quarter)].astype(BF16)

        @pl.when(t == f * per + c)
        def _():
            dbuf[t] = dcast[c]

        if c == 0:
            send_own(0, 1)

    @pl.when(side)
    def _():
        for h in DUAL:
            for c in range(per):
                o_copy(q - 1, c, h, toward).start()

    @pl.when(q == 3)
    def _():
        for c in range(per):
            o_copy(2, c, 0, fx).start()
            o_copy(2, c, 1, fy).start()

    for h in CHAIN + DUAL:
        for c in range(per):
            @pl.when(t != f * per + c)
            def _():
                dz_copy(c, h).start()

    @pl.when(q == 0)
    def _():
        own_chain()

    for w in range(2):
        cast(w, X_ORDER[1])
        cast(w, Y_ORDER[1])
        if w == 1:
            send_own(1, 0)
    send_own(1, 1)

    def arrive(step, w):
        i = X_ORDER[step]
        w_copy(w, fx, i, fwd_s.at[w, i], fy).wait_recv()
        i = Y_ORDER[step]
        w_copy(w, fy, i, fwd_s.at[w, i], fx).wait_recv()

    def forward(step, w):
        i = X_ORDER[step]
        w_copy(w, fx, i, fwd_s.at[w, i], fy).start()
        i = Y_ORDER[step]
        w_copy(w, fy, i, fwd_s.at[w, i], fx).start()

    def relay(way):
        h = 1 - way

        @pl.when(q == 1 + way)
        def _():
            for c in range(per):
                transit(c, h, toward).wait_recv()
                transit(c, h, toward).start()
                over_z(2, c, h, away).start()

    for w in range(2):
        with scope("arrive0"):
            arrive(0, w)
    with scope("transit"):
        relay(0)
        relay(1)
    for w in range(2):
        send_own(2, w)

    with scope("own_chain"):
        @pl.when(side)
        def _():
            own_chain()

    for w in range(2):
        send_own(3, w)

    with scope("over_z"):
        @pl.when(q == 0)
        def _():
            for h in DUAL:
                for c in range(per):
                    for slot, column in enumerate((fx, fy)):
                        o_copy(slot, c, h, fx).wait_recv()
                        over_z(slot, c, h, column).start()

    with scope("arrive1"):
        for w in range(2):
            forward(0, w)
        for w in range(2):
            arrive(1, w)
            forward(1, w)

    tile = 512

    def accumulate(src, first):
        def one(n, _):
            w, column = n // (wbuf.shape[3] // tile), pl.multiple_of(n % (wbuf.shape[3] // tile) * tile, tile)
            total = 0.0 if first else acc[w, :, pl.ds(column, tile)]
            for p in range(per):
                total = total + jnp.dot(
                    tbuf[src * per + p],
                    wbuf[w, src, pl.ds(p * width, width), pl.ds(column, tile)],
                    preferred_element_type=F32,
                )
            acc[w, :, pl.ds(column, tile)] = total
            return 0

        lax.fori_loop(0, 2 * (wbuf.shape[3] // tile), one, 0)

    with scope("over_z2"):
        @pl.when(q == 0)
        def _():
            for c in range(per):
                for h in DUAL:
                    o_copy(2, c, h, fx).wait_recv()
                    over_z(2, c, h, fd).start()

    with scope("tokens"):
        for slot, k in enumerate((2, 4, 6)):
            piece = flip(t, k)
            tok_copy(tbuf.at[piece], piece, 4 + slot, mate).wait_recv()
            tok_copy(tbuf.at[piece], piece, 4 + slot, mate).start()
        for k in (1, 3, 5, 7):
            tok_copy(tbuf.at[t], flip(t, k), 0, mate).wait_recv()

    with scope("own_chain3"):
        @pl.when(q == 3)
        def _():
            own_chain()

    def norm(i, _):
        block = pl.ds(i * piece_rows, piece_rows)
        squares = 0.0
        for p in range(n_tp):
            wide = tbuf[p, block].astype(F32)
            squares = squares + wide * wide
        scale[block] = lax.rsqrt(jnp.sum(squares, axis=1, keepdims=True) / (n_tp * width) + epsilon)
        return 0

    with scope("norm"):
        lax.fori_loop(0, n_tp, norm, 0)
    with scope("own_dot"):
        accumulate(f, True)
    with scope("arrive23"):
        for step in range(CHUNKS // 2, CHUNKS):
            for w in range(2):
                arrive(step, w)
    with scope("fx_dot"):
        accumulate(fx, False)
    with scope("fy_dot"):
        accumulate(fy, False)

    with scope("early"):
        @pl.when(q == 0)
        def _():
            for k in range(per, n_tp):
                for h in CHAIN:
                    chain(k, h)

        @pl.when(q == 1)
        def _():
            for k in (2, 3):
                for h in DUAL:
                    hand(k, h, fy)

        @pl.when(q == 2)
        def _():
            for k in (4, 5):
                for h in DUAL:
                    hand(k, h, fx)

        @pl.when(q == 3)
        def _():
            for k in (6, 7):
                hand(k, 0, fx)
                hand(k, 1, fy)

    with scope("fd_wait"):
        for i in (0, 2, 1, 3):
            for w in range(2):
                w_copy(w, fd, i, fwd_s.at[w, i], fx).wait_recv()
    with scope("fd_dot"):
        accumulate(fd, False)

    with scope("late"):
        @pl.when(q == 0)
        def _():
            for j in range(2):
                for h in DUAL:
                    hand(2 + j, h, fy)
                    hand(4 + j, h, fx)

    def make_hidden(n, _):
        columns = pl.ds(pl.multiple_of(n * tile, tile), tile)
        s = scale[...]
        g = acc[0, :, columns] * s
        hidden[:, columns] = (g / (1.0 + jnp.exp(-g)) * (acc[1, :, columns] * s)).astype(BF16)
        return 0

    with scope("hidden"):
        lax.fori_loop(0, hidden.shape[1] // tile, make_hidden, 0)

    def p_copy(k):
        return remote(psend.at[k], precv.at[k], p_s.at[k], p_r.at[k], f, mate)

    def z_copy(k, dz, piece):
        to = flip(t, 2 * dz)
        return remote(zsend.at[k, to // 2], zrecv.at[z, piece], z_s.at[k, dz], z_r.at[z, piece], f, to)

    def z_arrival(dz, piece):
        src = flip(t, 2 * dz)
        return remote(zsend.at[0, 0], zrecv.at[src // 2, piece], z_s.at[0, dz], z_r.at[src // 2, piece], f, src)

    def finish(k):
        p_copy(k).wait_recv()
        for b in range(n_z):
            block = (keep[flip(k, 1), b] + precv[k, b].astype(F32)).astype(BF16)
            zsend[k, b] = block
        piece = flip(mate, k)
        zrecv[z, piece] = zsend[k, z]
        for dz in range(1, n_z):
            z_copy(k, dz, piece).start()

    def product(k):
        piece = flip(t, k)
        out = jnp.dot(hidden[...], dbuf[piece], preferred_element_type=F32)
        out = out.reshape(n_z, 2, piece_rows, width)

        @pl.when(core == 0)
        def _():
            keep[k] = out[:, 0]
            psend[k] = out[:, 1].astype(BF16)

        @pl.when(core == 1)
        def _():
            keep[k] = out[:, 1]
            psend[k] = out[:, 0].astype(BF16)

        p_copy(k).start()

    def take(k):
        piece = flip(t, k)
        r = k // 2
        passed = jnp.logical_or(
            jnp.logical_or(jnp.logical_and(r == 1, q < 2), jnp.logical_and(r == 2, q % 2 == 0)),
            jnp.logical_and(r == 3, q == 3),
        )

        @pl.when(jnp.logical_and(r > 0, jnp.logical_not(passed)))
        def _():
            for h in DUAL:
                d_copy(piece, h, fx).wait_recv()

        for side_h in range(2):
            @pl.when(chain_stops[side_h])
            def _():
                d_copy(piece, CHAIN[side_h], fx).wait_recv()

                @pl.when(r == 0)
                def _():
                    d_copy(piece, DUAL[side_h], fx).wait_recv()

    def turn(i):
        j = i // 2
        one, two, three = [jnp.where(j == n, 1, 0) for n in (1, 2, 3)]
        first, second = jnp.where(q == 1, 1, 0), jnp.where(q == 2, 1, 0)
        return i + 2 * (first * (two - three) + second * (one + two - 2 * three))

    def step(i, _):
        @pl.when(jnp.logical_and(i % 2 == 0, i >= 2))
        def _():
            with scope("finish"):
                finish(turn(i - 2))
                finish(turn(i - 1))

        with scope("pass_on"):
            for role, lead in ((q == 3, 1), (side, 3)):
                @pl.when(jnp.logical_and(role, i == 2))
                def _():
                    for n in range(lead):
                        for h in CHAIN:
                            chain(i + n, h)

                @pl.when(jnp.logical_and(role, jnp.logical_and(i >= 2, i + lead < n_tp)))
                def _():
                    for h in CHAIN:
                        chain(i + lead, h)

        @pl.when(i < n_tp)
        def _():
            with scope("take"):
                take(turn(i))
            with scope("product"):
                product(turn(i))

        @pl.when(i == n_tp // 2)
        def _():
            with scope("sent"):
                for slot in range(4):
                    tok_copy(tbuf.at[t], t, slot, mate).wait_send()
                for slot in range(3):
                    tok_copy(tbuf.at[t], t, 4 + slot, mate).wait_send()
                for w in range(2):
                    for n in range(CHUNKS):
                        w_copy(w, f, n, own_s.at[0, w, n], fx).wait_send()
                        w_copy(w, f, n, own_s.at[1, w, n], fy).wait_send()
                        w_copy(w, f, n, fwd_s.at[w, n], fx).wait_send()
                for c in range(per):
                    for h in range(QUARTERS):
                        @pl.when(t != f * per + c)
                        def _():
                            dz_copy(c, h).wait_send()

                @pl.when(q != 0)
                def _():
                    for c in range(per):
                        for h in DUAL:
                            o_copy(2, c, h, fx).wait_send()

                @pl.when(q == 0)
                def _():
                    for slot in range(3):
                        for c in range(per):
                            for h in DUAL:
                                over_z(slot, c, h, f).wait_send()

                for way in range(2):
                    @pl.when(q == 1 + way)
                    def _():
                        for c in range(per):
                            transit(c, 1 - way, toward).wait_send()
                            over_z(2, c, 1 - way, away).wait_send()

        return 0

    lax.fori_loop(0, n_tp + 1, step, 0)

    with scope("sent2"):
        for k in range(n_tp):
            piece = flip(t, k)
            for h in range(QUARTERS):
                if k < per or h in CHAIN:
                    go = jnp.logical_not(chain_stops[h % 2])
                else:
                    go = (None, q < 2, q % 2 == 0, q == 3)[k // 2]

                @pl.when(go)
                def _():
                    d_copy(piece, h, fx).wait_send()
            p_copy(k).wait_send()

    for piece in range(n_tp):
        with scope("z_wait"):
            for dz in range(1, n_z):
                z_arrival(dz, piece).wait_recv()
        total = zrecv[0, piece].astype(F32)
        for b in range(1, n_z):
            total = total + zrecv[b, piece].astype(F32)
        layer_out[:, pl.ds(piece * width, width)] = total.astype(BF16)
    with scope("sent3"):
        for k in range(n_tp):
            for dz in range(1, n_z):
                z_copy(k, dz, k).wait_send()


def write_out(weights, down, layer, gate_out, up_out, down_out, layer_out, w_s, d_s, l_s):
    _, n_fs, rows, _ = weights.shape
    n_tp, _, width = down.shape
    copies = [pltpu.make_async_copy(layer, layer_out, l_s)]
    for w, out in enumerate((gate_out, up_out)):
        for src in range(n_fs):
            copies.append(pltpu.make_async_copy(weights.at[w, src], out.at[pl.ds(src * rows, rows)], w_s.at[w, src]))
    for j in range(n_tp):
        copies.append(pltpu.make_async_copy(down.at[j], down_out.at[:, pl.ds(j * width, width)], d_s.at[j]))
    for copy in copies:
        copy.start()
    for copy in copies:
        copy.wait()


def body(tokens, norm_gain, gate_train, up_train, down_train, *, n_fs, n_tp):
    n_tok, width = tokens.shape
    rows, cols = gate_train.shape
    tall = down_train.shape[0] * n_fs // n_tp
    piece_rows = n_tok // n_tp
    n_z = n_tp // 2
    hbm = pl.BlockSpec(memory_space=pltpu.HBM)
    vmem = pl.BlockSpec(memory_space=pltpu.VMEM)
    dma = pltpu.SemaphoreType.DMA
    weights, down, layer = pl.pallas_call(
        kernel,
        out_shape=(
            pltpu.VMEM((2, n_fs, rows, cols), BF16),
            pltpu.VMEM((n_tp, tall, width), BF16),
            pltpu.VMEM((piece_rows, width * n_tp), BF16),
        ),
        in_specs=[hbm] * 5,
        out_specs=(vmem, vmem, vmem),
        scratch_shapes=[
            pltpu.VMEM((1, rows), F32),
            pltpu.VMEM((2, rows, cols), F32),
            pltpu.VMEM(down_train.shape, F32),
            pltpu.VMEM((n_tp // n_fs, tall, width), BF16),
            pltpu.VMEM((3, n_tp // n_fs, tall // QUARTERS * len(DUAL), width), BF16),
            pltpu.VMEM((n_tp, n_tok, width), BF16),
            pltpu.VMEM((2, n_tok, cols), F32),
            pltpu.VMEM((n_tok, cols), BF16),
            pltpu.VMEM((n_tok, 1), F32),
            pltpu.VMEM((n_tp, n_z, piece_rows, width), F32),
            pltpu.VMEM((n_tp, n_z, piece_rows, width), BF16),
            pltpu.VMEM((n_tp, n_z, piece_rows, width), BF16),
            pltpu.VMEM((n_tp, n_z, piece_rows, width), BF16),
            pltpu.VMEM((n_z, n_tp, piece_rows, width), BF16),
            dma,
            dma,
            dma((2, CHUNKS)),
            dma((n_tp // n_fs,)),
            dma((7,)),
            dma((n_tp,)),
            dma((2, 2, CHUNKS)),
            dma((2, CHUNKS)),
            dma((2, n_fs, CHUNKS)),
            dma((n_tp // n_fs, QUARTERS)),
            dma((2, n_tp // n_fs, len(DUAL))),
            dma((3, n_tp // n_fs, len(DUAL))),
            dma((3, n_tp // n_fs, len(DUAL))),
            dma((n_tp, QUARTERS)),
            dma((n_tp, QUARTERS)),
            dma((n_tp,)),
            dma((n_tp,)),
            dma((n_tp, n_z)),
            dma((n_z, n_tp)),
        ],
        compiler_params=pltpu.CompilerParams(
            collective_id=0, has_side_effects=True, vmem_limit_bytes=51 * 1024 * 1024
        ),
    )(tokens, norm_gain[None, :], gate_train, up_train, down_train)
    return pl.pallas_call(
        write_out,
        out_shape=(
            jax.ShapeDtypeStruct((rows * n_fs, cols), BF16),
            jax.ShapeDtypeStruct((rows * n_fs, cols), BF16),
            jax.ShapeDtypeStruct((tall, width * n_tp), BF16),
            jax.ShapeDtypeStruct((piece_rows, width * n_tp), BF16),
        ),
        in_specs=[vmem] * 3,
        out_specs=(pl.BlockSpec(memory_space=pl.ANY),) * 4,
        scratch_shapes=[dma((2, n_fs)), dma((n_tp,)), dma],
        compiler_params=pltpu.CompilerParams(vmem_limit_bytes=4 * 1024 * 1024),
    )(weights, down, layer)


def plain(tokens, norm_gain, gate_train, up_train, down_train):
    gate_local = (norm_gain[:, None] * gate_train).astype(BF16)
    up_local = (norm_gain[:, None] * up_train).astype(BF16)
    down_local = down_train.astype(BF16)
    features = lax.all_gather(tokens, "tp", axis=1, tiled=True)
    wide = features.astype(F32)
    squares = jnp.sum(wide * wide, axis=1)
    gate_whole = lax.all_gather(gate_local, "fs", axis=0, tiled=True)
    up_whole = lax.all_gather(up_local, "fs", axis=0, tiled=True)
    gate_sum = jnp.dot(features, gate_whole, preferred_element_type=F32)
    up_sum = jnp.dot(features, up_whole, preferred_element_type=F32)
    down_rows = lax.all_gather(down_local, "fs", axis=0, tiled=True)
    down_whole = lax.all_to_all(down_rows, "tp", split_axis=0, concat_axis=1, tiled=True)
    scale = lax.rsqrt(squares / features.shape[1] + epsilon)[:, None]
    hidden = (jax.nn.silu(gate_sum * scale) * (up_sum * scale)).astype(BF16)
    mixed = lax.psum_scatter(
        jnp.dot(hidden, down_whole, preferred_element_type=F32).astype(BF16), "tp", scatter_dimension=0, tiled=True
    )
    return (gate_whole, up_whole, down_whole, mixed)


def solution(mesh):
    n_fs, n_tp = mesh.shape["fs"], mesh.shape["tp"]
    fast = n_fs == 4 and n_tp == 8
    return jax.shard_map(
        functools.partial(body, n_fs=n_fs, n_tp=n_tp) if fast else plain,
        mesh=mesh,
        in_specs=(P("fs", "tp"), P("fs"), P("fs", "tp"), P("fs", "tp"), P("fs", "tp")),
        out_specs=(P(None, "tp"), P(None, "tp"), P("tp", None), P(("fs", "tp"), None)),
        check_vma=False,
    )
```

time: 154 us -> 144 us (0.935); the launches traced: 154 us -> 141 us
  Pallas kernels: 148 us -> 140 us
  local copies, waits for them, and re-layouts: 4.95 us -> 0 us
    pallas_call x1, Pallas kernels: 144 us -> 136 us  [body(): pl.pallas_call(kernel, out_shape=(pltpu.VMEM((2, n_fs, rows, cols), BF16)...]
    unnamed x6 -> x0, local copies, waits for them, and re-layouts: 4.13 us -> none
where the time goes in v1:
time: 144 us; the launch traced here: 141 us
  Pallas kernels  140 us (97%)
    pallas_call x1, Pallas kernels, body(): pl.pallas_call(kernel, out_shape=(pltpu.VMEM((2, n_fs, rows, cols), BF16)...  136 us
    pallas_call x1, Pallas kernels, body(): pl.pallas_call(write_out, out_shape=(jax.ShapeDtypeStruct((rows * n_fs, c...  4.77 us

profile of v1, /device:TPU:0, one launch (start us, length us, event | category | flops | bytes accessed | tf_op | source)
XLA Modules:
  0.0 141.1 jit_solution(11787037242485001276)
XLA Ops:
  0.6 135.7 %shard_map.84 = (bf16[2,4,512,1024]{3,2,1,0:T(8,128)(2,1)S(1)}, bf16[8,1024,256]{2,1,0:T(8,128)(2,1)S(1)}, bf16[64,2048]{1,0:T(8,128)(2,1)S(1)}) custom-call(bf16[512,256]{1,0:T(8,128)(2,1)} %tok_in.1, f32[1,512]{1,0:T(1,128)} %bitcast.1, f32[512,1024]{1,0:T(8,128)} %gate_in.1, f32[512,1024]{1,0:T(8,128)} %up_in.1, f32[2048,256]{1,0:T(8,128)} %down_in.1), custom_call_target="tpu_custom_call" | custom-call | tf_op jit(solution)/shard_map/pallas_call | solution.py:559
  136.3 4.8 %shard_map.85 = (bf16[2048,1024]{1,0:T(8,128)(2,1)}, bf16[2048,1024]{1,0:T(8,128)(2,1)}, bf16[1024,2048]{1,0:T(8,128)(2,1)}, bf16[64,2048]{1,0:T(8,128)(2,1)}) custom-call(bf16[2,4,512,1024]{3,2,1,0:T(8,128)(2,1)S(1)} %get-tuple-element.7.weights, bf16[8,1024,256]{2,1,0:T(8,128)(2,1)S(1)} %get-tuple-element.8.down, bf16[64,2048]{1,0:T(8,128)(2,1)S(1)} %get-tuple-element.9.layer), custom_call_target="tpu_custom_call" | custom-call | tf_op jit(solution)/shard_map/pallas_call | solution.py:607

commit v2 on v1

v2 whole, which is shorter than its diff:
```python
import functools

import jax
import jax.numpy as jnp
from jax import lax
from jax.experimental import pallas as pl
from jax.experimental.pallas import tpu as pltpu
from jax.sharding import PartitionSpec as P

MESH = pl.DeviceIdType.MESH
BF16 = jnp.bfloat16
F32 = jnp.float32
epsilon = 1e-06
CHUNKS = 4
X_ORDER = (0, 1, 2, 3)
Y_ORDER = (2, 3, 0, 1)
QUARTERS = 4
DUAL = (0, 1)
CHAIN = (2, 3)
scope = jax.named_scope


def flip(a, k):
    result = 0
    for bit in (1, 2, 4):
        own, other = (a // bit) % 2, (k // bit) % 2
        result = result + bit * (own + other - 2 * own * other)
    return result


def kernel(
    tok_in, gain_in, gate_in, up_in, down_in,
    wbuf, dbuf, layer_out,
    gain, w32, d32, dcast, xbuf, tbuf, acc, hidden, scale, keep, psend, precv, zsend, zrecv,
    load_g, load_t, load_w, load_d, tok_s, tok_r, w_s, w_r, dz_s, o_s, o_r, zr_s, d_s, d_r, p_s, p_r, z_s, z_r,
):
    f, t = lax.axis_index("fs"), lax.axis_index("tp")
    n_tp, n_fs = tbuf.shape[0], wbuf.shape[1]
    z, core = t // 2, t % 2
    fx, fy, fd = flip(f, 1), flip(f, 2), flip(f, 3)
    mate = flip(t, 1)
    base = t - core
    rows = wbuf.shape[2]
    part = rows // CHUNKS
    w_ins = (gate_in, up_in)
    tall, width = dbuf.shape[1], dbuf.shape[2]
    quarter = tall // QUARTERS
    per = n_tp // n_fs
    n_tok = tbuf.shape[1]
    piece_rows = n_tok // n_tp
    n_z = n_tp // 2
    q = flip(f, z)
    side = jnp.logical_or(q == 1, q == 2)
    toward = fx + (fy - fx) * (q // 2)
    away = fy + (fx - fy) * (q // 2)

    def remote(src, dst, ss, rs, to_f, to_t):
        return pltpu.make_async_remote_copy(
            src_ref=src, dst_ref=dst, send_sem=ss, recv_sem=rs, device_id=(to_f, to_t), device_id_type=MESH
        )

    def load(w, i):
        return pltpu.make_async_copy(w_ins[w].at[pl.ds(i * part, part)], w32.at[w, pl.ds(i * part, part)], load_w.at[w, i])

    barrier = pltpu.get_barrier_semaphore()
    peers = [(fx, t), (fy, t)] + [(f, flip(t, k)) for k in range(1, n_tp)]
    for peer in peers:
        pl.semaphore_signal(barrier, inc=1, device_id=peer, device_id_type=MESH)

    load_gain = pltpu.make_async_copy(gain_in, gain, load_g)
    load_tok = pltpu.make_async_copy(tok_in, tbuf.at[t], load_t)
    load_down = [
        pltpu.make_async_copy(down_in.at[pl.ds(c * tall, tall)], d32.at[pl.ds(c * tall, tall)], load_d.at[c])
        for c in range(per)
    ]
    load_gain.start()
    for i in (0, 2):
        for w in range(2):
            load(w, i).start()
    load_tok.start()
    for copy in load_down:
        copy.start()
    for i in (1, 3):
        for w in range(2):
            load(w, i).start()

    def cast(w, i):
        block = pl.ds(i * part, part)
        load(w, i).wait()
        lanes = 128
        tall_gain = jnp.broadcast_to(gain[:, block], (lanes, part)).T
        for j in range(wbuf.shape[3] // lanes):
            columns = pl.ds(j * lanes, lanes)
            wbuf[w, f, block, columns] = (tall_gain * w32[w, block, columns]).astype(BF16)

    def tok_copy(piece, dz, to):
        return remote(tbuf.at[piece], tbuf.at[piece], tok_s, tok_r.at[dz], f, to)

    def w_copy(src, i, to):
        ref = wbuf.at[:, src, pl.ds(i * part, part)]
        return remote(ref, ref, w_s, w_r.at[src, i], to, t)

    def send_own(step):
        w_copy(f, X_ORDER[step], fx).start()
        w_copy(f, Y_ORDER[step], fy).start()

    def rows_of(h):
        return pl.ds(h * quarter, quarter)

    def dz_copy(c, h):
        return remote(dcast.at[c, rows_of(h)], dbuf.at[t, rows_of(h)], dz_s, d_r.at[t, h], f, f * per + c)

    def o_copy(slot, h, to):
        return remote(dcast.at[:, rows_of(h)], xbuf.at[slot, :, rows_of(h)], o_s, o_r.at[slot, h], to, t)

    def transit(h, to):
        ref = xbuf.at[2, :, rows_of(h)]
        return remote(ref, ref, o_s, o_r.at[2, h], to, t)

    def over_z(slot, c, h, column):
        return remote(xbuf.at[slot, c, rows_of(h)], dbuf.at[t, rows_of(h)], zr_s, d_r.at[t, h], f, column * per + c)

    def d_copy(piece, h, to):
        ref = dbuf.at[piece, rows_of(h)]
        return remote(ref, ref, d_s, d_r.at[piece, h], to, t)

    def sent(ref, sem):
        remote(ref, ref, sem, sem, fx, t).wait_send()

    chain_stops = (q == 2, q == 1)
    chain_to = (fx + (fy - fx) * (q % 2) * (1 - q // 2), fy + (fx - fy) * (1 - q % 2) * (q // 2))

    def chain(k, hs):
        piece = flip(base, k)
        for h in hs:
            @pl.when(jnp.logical_not(chain_stops[h % 2]))
            def _():
                if isinstance(k, int) and k < per:
                    @pl.when(jnp.logical_or(q != 0, core != k))
                    def _():
                        d_copy(piece, h, chain_to[h % 2]).wait_recv()
                else:
                    d_copy(piece, h, chain_to[h % 2]).wait_recv()
                d_copy(piece, h, chain_to[h % 2]).start()

    inner = jnp.logical_or(z == 1, z == 2)

    def chain_next(n):
        r = n // 2
        chain(2 * jnp.where(inner, 1 + r, 3 - r) + n % 2, CHAIN)

    def own_chain():
        for k in range(per):
            chain(k, range(QUARTERS))

    def hand(k, h, to):
        piece = flip(base, k)
        d_copy(piece, h, to).wait_recv()
        d_copy(piece, h, to).start()

    load_gain.wait()
    cast(0, X_ORDER[0])
    cast(0, Y_ORDER[0])
    cast(1, X_ORDER[0])
    cast(1, Y_ORDER[0])
    with scope("barrier"):
        pl.semaphore_wait(barrier, len(peers))
    send_own(0)
    load_tok.wait()
    for dz, k in enumerate((1, 2, 4, 6)):
        tok_copy(t, dz, flip(t, k)).start()

    for c in range(per):
        load_down[c].wait()
        for h in range(QUARTERS):
            dcast[c, rows_of(h)] = d32[pl.ds(c * tall + h * quarter, quarter)].astype(BF16)

        @pl.when(t == f * per + c)
        def _():
            dbuf[t] = dcast[c]

    cast(0, X_ORDER[1])
    cast(0, Y_ORDER[1])

    @pl.when(side)
    def _():
        for h in DUAL:
            o_copy(q - 1, h, toward).start()

    @pl.when(q == 3)
    def _():
        o_copy(2, 0, fx).start()
        o_copy(2, 1, fy).start()

    for h in CHAIN + DUAL:
        for c in range(per):
            @pl.when(t != f * per + c)
            def _():
                dz_copy(c, h).start()

    cast(1, X_ORDER[1])
    cast(1, Y_ORDER[1])

    @pl.when(q == 0)
    def _():
        own_chain()

    send_own(1)

    def arrive(step):
        w_copy(fx, X_ORDER[step], fy).wait_recv()
        w_copy(fy, Y_ORDER[step], fx).wait_recv()

    def forward(step):
        w_copy(fx, X_ORDER[step], fy).start()
        w_copy(fy, Y_ORDER[step], fx).start()

    with scope("arrive0"):
        arrive(0)
    with scope("transit"):
        for way in range(2):
            @pl.when(q == 1 + way)
            def _():
                transit(1 - way, toward).wait_recv()
                transit(1 - way, toward).start()
                for c in range(per):
                    over_z(2, c, 1 - way, away).start()

    send_own(2)

    with scope("own_chain"):
        @pl.when(side)
        def _():
            own_chain()

    send_own(3)

    with scope("over_z"):
        @pl.when(q == 0)
        def _():
            for h in DUAL:
                for slot, column in enumerate((fx, fy)):
                    o_copy(slot, h, fx).wait_recv()
                    for c in range(per):
                        over_z(slot, c, h, column).start()

    with scope("arrive1"):
        forward(0)
        arrive(1)

    with scope("over_z2"):
        @pl.when(q == 0)
        def _():
            for h in DUAL:
                o_copy(2, h, fx).wait_recv()
                for c in range(per):
                    over_z(2, c, h, fd).start()

    with scope("chain0"):
        @pl.when(q == 0)
        def _():
            chain_next(0)
            chain_next(1)

    forward(1)

    tile = 512

    def accumulate(src, first):
        def one(n, _):
            w, column = n // (wbuf.shape[3] // tile), pl.multiple_of(n % (wbuf.shape[3] // tile) * tile, tile)
            total = 0.0 if first else acc[w, :, pl.ds(column, tile)]
            for p in range(per):
                total = total + jnp.dot(
                    tbuf[src * per + p],
                    wbuf[w, src, pl.ds(p * width, width), pl.ds(column, tile)],
                    preferred_element_type=F32,
                )
            acc[w, :, pl.ds(column, tile)] = total
            return 0

        lax.fori_loop(0, 2 * (wbuf.shape[3] // tile), one, 0)

    with scope("tokens"):
        for dz in range(1, n_z):
            piece = flip(t, 2 * dz)
            tok_copy(piece, dz, mate).wait_recv()
            tok_copy(piece, 0, mate).start()
        remote(tbuf.at[pl.ds(0, n_z)], tbuf.at[pl.ds(0, n_z)], tok_s, tok_r.at[0], f, mate).wait_recv()

    with scope("own_chain3"):
        @pl.when(q == 3)
        def _():
            own_chain()

    def norm(i, _):
        block = pl.ds(i * piece_rows, piece_rows)
        squares = 0.0
        for p in range(n_tp):
            wide = tbuf[p, block].astype(F32)
            squares = squares + wide * wide
        scale[block] = lax.rsqrt(jnp.sum(squares, axis=1, keepdims=True) / (n_tp * width) + epsilon)
        return 0

    with scope("norm"):
        lax.fori_loop(0, n_tp, norm, 0)
    with scope("own_dot"):
        accumulate(f, True)
    with scope("arrive23"):
        for step in range(CHUNKS // 2, CHUNKS):
            arrive(step)
    with scope("fx_dot"):
        accumulate(fx, False)
    with scope("fy_dot"):
        accumulate(fy, False)

    with scope("early"):
        @pl.when(q == 0)
        def _():
            for n in range(2, 6):
                chain_next(n)

        for place, k, to in ((1, 2, fy), (2, 4, fx)):
            @pl.when(q == place)
            def _():
                chain_next(0)
                chain_next(1)
                for h in DUAL:
                    hand(k, h, to)
                    d_copy(flip(base, k + 1), h, to).wait_recv()

        @pl.when(q == 3)
        def _():
            hand(6, 0, fx)
            hand(6, 1, fy)

    with scope("fd_wait"):
        for i in range(CHUNKS):
            w_copy(fd, i, fx).wait_recv()
    with scope("fd_dot"):
        accumulate(fd, False)

    with scope("late"):
        @pl.when(q == 0)
        def _():
            for j in range(2):
                for h in DUAL:
                    hand(2 + j, h, fy)
                    hand(4 + j, h, fx)

    def make_hidden(n, _):
        columns = pl.ds(pl.multiple_of(n * tile, tile), tile)
        s = scale[...]
        g = acc[0, :, columns] * s
        hidden[:, columns] = (g / (1.0 + jnp.exp(-g)) * (acc[1, :, columns] * s)).astype(BF16)
        return 0

    with scope("hidden"):
        lax.fori_loop(0, hidden.shape[1] // tile, make_hidden, 0)

    def p_copy(k):
        return remote(psend.at[k], precv.at[k], p_s, p_r.at[k], f, mate)

    def z_copy(k, dz, piece):
        to = flip(t, 2 * dz)
        return remote(zsend.at[k, to // 2], zrecv.at[z, piece], z_s, z_r.at[piece], f, to)

    def finish(k):
        p_copy(k).wait_recv()
        for b in range(n_z):
            zsend[k, b] = (keep[k, b] + precv[k, b].astype(F32)).astype(BF16)
        piece = flip(base, k)
        zrecv[z, piece] = zsend[k, z]
        for dz in range(1, n_z):
            z_copy(k, dz, piece).start()

    def product(k):
        piece = flip(base, k)
        out = jnp.dot(hidden[...], dbuf[piece], preferred_element_type=F32)
        out = out.reshape(n_z, 2, piece_rows, width)

        @pl.when(core == 0)
        def _():
            keep[k] = out[:, 0]
            psend[k] = out[:, 1].astype(BF16)

        @pl.when(core == 1)
        def _():
            keep[k] = out[:, 1]
            psend[k] = out[:, 0].astype(BF16)

        p_copy(k).start()

    def take(k):
        piece = flip(base, k)
        r = k // 2
        passed = jnp.logical_or(
            jnp.logical_or(jnp.logical_and(r == 1, q < 2), jnp.logical_and(r == 2, q % 2 == 0)),
            jnp.logical_and(r == 3, q == 3),
        )

        @pl.when(jnp.logical_and(r > 0, jnp.logical_not(passed)))
        def _():
            for h in DUAL:
                d_copy(piece, h, fx).wait_recv()

        for side_h in range(2):
            @pl.when(chain_stops[side_h])
            def _():
                d_copy(piece, CHAIN[side_h], fx).wait_recv()

                @pl.when(r == 0)
                def _():
                    d_copy(piece, DUAL[side_h], fx).wait_recv()

    def turn(i):
        k = i
        for here, order in (
            (jnp.logical_and(inner, q == 2), (0, 1, 4, 2, 5, 6, 3, 7)),
            (jnp.logical_and(inner, q == 3), (0, 1, 2, 4, 6, 7, 3, 5)),
            (jnp.logical_and(jnp.logical_not(inner), q % 2 == 0), (0, 1, 6, 7, 4, 5, 2, 3)),
            (jnp.logical_and(jnp.logical_not(inner), q % 2 == 1), (0, 1, 6, 7, 4, 2, 5, 3)),
        ):
            mine = 0
            for n, v in enumerate(order):
                mine = mine + v * jnp.where(i == n, 1, 0)
            k = jnp.where(here, mine, k)
        return k

    def pass_on(i):
        @pl.when(jnp.logical_and(side, i == 2))
        def _():
            chain_next(i)

        @pl.when(jnp.logical_and(side, jnp.logical_and(i >= 2, i <= 4)))
        def _():
            chain_next(i + 1)

        for place, k, to in ((1, 3, fy), (2, 5, fx)):
            @pl.when(jnp.logical_and(q == place, i == 4))
            def _():
                for h in DUAL:
                    d_copy(flip(base, k), h, to).start()

        @pl.when(jnp.logical_and(q == 3, i == 2))
        def _():
            chain_next(i - 2)
            chain_next(i - 1)
            hand(7, 0, fx)
            hand(7, 1, fy)

        @pl.when(jnp.logical_and(q == 3, jnp.logical_and(i >= 3, i <= 4)))
        def _():
            chain_next(i - 1)

        @pl.when(jnp.logical_and(q == 3, jnp.logical_and(i >= 4, i <= 5)))
        def _():
            chain_next(i)

    def step(i, _):
        with scope("pass_on"):
            pass_on(i)

        @pl.when(i >= 1)
        def _():
            with scope("finish"):
                finish(turn(i - 1))

        @pl.when(i < n_tp)
        def _():
            k = turn(i)
            with scope("take"):
                take(k)
            with scope("product"):
                product(k)

        return 0

    lax.fori_loop(0, n_tp + 1, step, 0)

    with scope("sent"):
        sent(tbuf.at[pl.ds(0, n_tp - 1)], tok_s)
        sent(wbuf.at[:, pl.ds(0, n_fs - 1)], w_s)
        sent(psend, p_s)

        @pl.when(q == 0)
        def _():
            sent(dcast.at[0], dz_s)
            sent(xbuf, zr_s)
            sent(dbuf.at[pl.ds(0, 7)], d_s)

        @pl.when(side)
        def _():
            sent(xbuf.at[:, :, rows_of(0)], o_s)
            sent(xbuf.at[0, 0], zr_s)
            sent(dbuf.at[pl.ds(0, 7), pl.ds(0, 2 * quarter)], d_s)

        @pl.when(q == 3)
        def _():
            sent(xbuf.at[0], o_s)
            sent(dbuf.at[pl.ds(0, 6)], d_s)

        @pl.when(q != 0)
        def _():
            sent(dcast, dz_s)

    for piece in range(n_tp):
        with scope("z_wait"):
            others = zrecv.at[pl.ds(0, n_z - 1), piece]
            remote(others, others, z_s, z_r.at[piece], f, mate).wait_recv()
        total = zrecv[0, piece].astype(F32)
        for b in range(1, n_z):
            total = total + zrecv[b, piece].astype(F32)
        layer_out[:, pl.ds(piece * width, width)] = total.astype(BF16)
    sent(zsend.at[:, pl.ds(0, n_z - 1)], z_s)


def write_out(weights, down, layer, gate_out, up_out, down_out, layer_out, w_s, d_s, l_s):
    _, n_fs, rows, _ = weights.shape
    n_tp, _, width = down.shape
    copies = [pltpu.make_async_copy(layer, layer_out, l_s)]
    for w, out in enumerate((gate_out, up_out)):
        for src in range(n_fs):
            copies.append(pltpu.make_async_copy(weights.at[w, src], out.at[pl.ds(src * rows, rows)], w_s.at[w, src]))
    for j in range(n_tp):
        copies.append(pltpu.make_async_copy(down.at[j], down_out.at[:, pl.ds(j * width, width)], d_s.at[j]))
    for copy in copies:
        copy.start()
    for copy in copies:
        copy.wait()


def body(tokens, norm_gain, gate_train, up_train, down_train, *, n_fs, n_tp):
    n_tok, width = tokens.shape
    rows, cols = gate_train.shape
    tall = down_train.shape[0] * n_fs // n_tp
    piece_rows = n_tok // n_tp
    n_z = n_tp // 2
    hbm = pl.BlockSpec(memory_space=pltpu.HBM)
    vmem = pl.BlockSpec(memory_space=pltpu.VMEM)
    dma = pltpu.SemaphoreType.DMA
    weights, down, layer = pl.pallas_call(
        kernel,
        out_shape=(
            pltpu.VMEM((2, n_fs, rows, cols), BF16),
            pltpu.VMEM((n_tp, tall, width), BF16),
            pltpu.VMEM((piece_rows, width * n_tp), BF16),
        ),
        in_specs=[hbm] * 5,
        out_specs=(vmem, vmem, vmem),
        scratch_shapes=[
            pltpu.VMEM((1, rows), F32),
            pltpu.VMEM((2, rows, cols), F32),
            pltpu.VMEM(down_train.shape, F32),
            pltpu.VMEM((n_tp // n_fs, tall, width), BF16),
            pltpu.VMEM((3, n_tp // n_fs, tall // QUARTERS * len(DUAL), width), BF16),
            pltpu.VMEM((n_tp, n_tok, width), BF16),
            pltpu.VMEM((2, n_tok, cols), F32),
            pltpu.VMEM((n_tok, cols), BF16),
            pltpu.VMEM((n_tok, 1), F32),
            pltpu.VMEM((n_tp, n_z, piece_rows, width), F32),
            pltpu.VMEM((n_tp, n_z, piece_rows, width), BF16),
            pltpu.VMEM((n_tp, n_z, piece_rows, width), BF16),
            pltpu.VMEM((n_tp, n_z, piece_rows, width), BF16),
            pltpu.VMEM((n_z, n_tp, piece_rows, width), BF16),
            dma,
            dma,
            dma((2, CHUNKS)),
            dma((n_tp // n_fs,)),
            dma,
            dma((n_z,)),
            dma,
            dma((n_fs, CHUNKS)),
            dma,
            dma,
            dma((3, len(DUAL))),
            dma,
            dma,
            dma((n_tp, QUARTERS)),
            dma,
            dma((n_tp,)),
            dma,
            dma((n_tp,)),
        ],
        compiler_params=pltpu.CompilerParams(
            collective_id=0, has_side_effects=True, vmem_limit_bytes=51 * 1024 * 1024
        ),
    )(tokens, norm_gain[None, :], gate_train, up_train, down_train)
    return pl.pallas_call(
        write_out,
        out_shape=(
            jax.ShapeDtypeStruct((rows * n_fs, cols), BF16),
            jax.ShapeDtypeStruct((rows * n_fs, cols), BF16),
            jax.ShapeDtypeStruct((tall, width * n_tp), BF16),
            jax.ShapeDtypeStruct((piece_rows, width * n_tp), BF16),
        ),
        in_specs=[vmem] * 3,
        out_specs=(pl.BlockSpec(memory_space=pl.ANY),) * 4,
        scratch_shapes=[dma((2, n_fs)), dma((n_tp,)), dma],
        compiler_params=pltpu.CompilerParams(vmem_limit_bytes=4 * 1024 * 1024),
    )(weights, down, layer)


def plain(tokens, norm_gain, gate_train, up_train, down_train):
    gate_local = (norm_gain[:, None] * gate_train).astype(BF16)
    up_local = (norm_gain[:, None] * up_train).astype(BF16)
    down_local = down_train.astype(BF16)
    features = lax.all_gather(tokens, "tp", axis=1, tiled=True)
    wide = features.astype(F32)
    squares = jnp.sum(wide * wide, axis=1)
    gate_whole = lax.all_gather(gate_local, "fs", axis=0, tiled=True)
    up_whole = lax.all_gather(up_local, "fs", axis=0, tiled=True)
    gate_sum = jnp.dot(features, gate_whole, preferred_element_type=F32)
    up_sum = jnp.dot(features, up_whole, preferred_element_type=F32)
    down_rows = lax.all_gather(down_local, "fs", axis=0, tiled=True)
    down_whole = lax.all_to_all(down_rows, "tp", split_axis=0, concat_axis=1, tiled=True)
    scale = lax.rsqrt(squares / features.shape[1] + epsilon)[:, None]
    hidden = (jax.nn.silu(gate_sum * scale) * (up_sum * scale)).astype(BF16)
    mixed = lax.psum_scatter(
        jnp.dot(hidden, down_whole, preferred_element_type=F32).astype(BF16), "tp", scatter_dimension=0, tiled=True
    )
    return (gate_whole, up_whole, down_whole, mixed)


def solution(mesh):
    n_fs, n_tp = mesh.shape["fs"], mesh.shape["tp"]
    fast = n_fs == 4 and n_tp == 8
    return jax.shard_map(
        functools.partial(body, n_fs=n_fs, n_tp=n_tp) if fast else plain,
        mesh=mesh,
        in_specs=(P("fs", "tp"), P("fs"), P("fs", "tp"), P("fs", "tp"), P("fs", "tp")),
        out_specs=(P(None, "tp"), P(None, "tp"), P("tp", None), P(("fs", "tp"), None)),
        check_vma=False,
    )
```

time: 144 us -> 132 us (0.917); the launches traced: 141 us -> 132 us
  Pallas kernels: 140 us -> 131 us
    pallas_call x1, Pallas kernels: 136 us -> 126 us  [body(): pl.pallas_call(kernel, out_shape=(pltpu.VMEM((2, n_fs, rows, cols), BF16)...]
where the time goes in v2:
time: 132 us
  Pallas kernels  131 us (99%)
    pallas_call x1, Pallas kernels, body(): pl.pallas_call(kernel, out_shape=(pltpu.VMEM((2, n_fs, rows, cols), BF16)...  126 us
    pallas_call x1, Pallas kernels, body(): pl.pallas_call(write_out, out_shape=(jax.ShapeDtypeStruct((rows * n_fs, c...  4.77 us

profile of v2, /device:TPU:0, one launch (start us, length us, event | category | flops | bytes accessed | tf_op | source)
XLA Modules:
  0.0 131.6 jit_solution(13448643464596200134)
XLA Ops:
  0.6 126.2 %shard_map.84 = (bf16[2,4,512,1024]{3,2,1,0:T(8,128)(2,1)S(1)}, bf16[8,1024,256]{2,1,0:T(8,128)(2,1)S(1)}, bf16[64,2048]{1,0:T(8,128)(2,1)S(1)}) custom-call(bf16[512,256]{1,0:T(8,128)(2,1)} %tok_in.1, f32[1,512]{1,0:T(1,128)} %bitcast.1, f32[512,1024]{1,0:T(8,128)} %gate_in.1, f32[512,1024]{1,0:T(8,128)} %up_in.1, f32[2048,256]{1,0:T(8,128)} %down_in.1), custom_call_target="tpu_custom_call" | custom-call | tf_op jit(solution)/shard_map/pallas_call | solution.py:542
  126.8 4.8 %shard_map.85 = (bf16[2048,1024]{1,0:T(8,128)(2,1)}, bf16[2048,1024]{1,0:T(8,128)(2,1)}, bf16[1024,2048]{1,0:T(8,128)(2,1)}, bf16[64,2048]{1,0:T(8,128)(2,1)}) custom-call(bf16[2,4,512,1024]{3,2,1,0:T(8,128)(2,1)S(1)} %get-tuple-element.7.weights, bf16[8,1024,256]{2,1,0:T(8,128)(2,1)S(1)} %get-tuple-element.8.down, bf16[64,2048]{1,0:T(8,128)(2,1)S(1)} %get-tuple-element.9.layer), custom_call_target="tpu_custom_call" | custom-call | tf_op jit(solution)/shard_map/pallas_call | solution.py:589

commit v3 on v2

--- a/solution.py
+++ b/solution.py
@@ -12,9 +12,10 @@
 F32 = jnp.float32
 epsilon = 1e-06
 CHUNKS = 4
-X_ORDER = (0, 1, 2, 3)
-Y_ORDER = (2, 3, 0, 1)
+X_ORDER = (0, 2, 1, 3)
+Y_ORDER = (1, 3, 0, 2)
 QUARTERS = 4
+CHAIN_SHARE = 2
 DUAL = (0, 1)
 CHAIN = (2, 3)
 scope = jax.named_scope
@@ -44,7 +45,8 @@
     part = rows // CHUNKS
     w_ins = (gate_in, up_in)
     tall, width = dbuf.shape[1], dbuf.shape[2]
-    quarter = tall // QUARTERS
+    short = tall * CHAIN_SHARE // 16
+    long = tall // 2 - short
     per = n_tp // n_fs
     n_tok = tbuf.shape[1]
     piece_rows = n_tok // n_tp
@@ -74,13 +76,13 @@
         for c in range(per)
     ]
     load_gain.start()
-    for i in (0, 2):
+    for i in (0, 1):
         for w in range(2):
             load(w, i).start()
     load_tok.start()
     for copy in load_down:
         copy.start()
-    for i in (1, 3):
+    for i in (2, 3):
         for w in range(2):
             load(w, i).start()
 
@@ -100,12 +102,18 @@
         ref = wbuf.at[:, src, pl.ds(i * part, part)]
         return remote(ref, ref, w_s, w_r.at[src, i], to, t)
 
+    def send_x(step):
+        w_copy(f, X_ORDER[step], fx).start()
+
+    def send_y(step):
+        w_copy(f, Y_ORDER[step], fy).start()
+
     def send_own(step):
-        w_copy(f, X_ORDER[step], fx).start()
-        w_copy(f, Y_ORDER[step], fy).start()
+        send_x(step)
+        send_y(step)
 
     def rows_of(h):
-        return pl.ds(h * quarter, quarter)
+        return pl.ds(h * long, long) if h in DUAL else pl.ds(2 * long + (h - 2) * short, short)
 
     def dz_copy(c, h):
         return remote(dcast.at[c, rows_of(h)], dbuf.at[t, rows_of(h)], dz_s, d_r.at[t, h], f, f * per + c)
@@ -160,12 +168,13 @@
 
     load_gain.wait()
     cast(0, X_ORDER[0])
-    cast(0, Y_ORDER[0])
     cast(1, X_ORDER[0])
-    cast(1, Y_ORDER[0])
     with scope("barrier"):
         pl.semaphore_wait(barrier, len(peers))
-    send_own(0)
+    cast(0, Y_ORDER[0])
+    send_x(0)
+    cast(1, Y_ORDER[0])
+    send_y(0)
     load_tok.wait()
     for dz, k in enumerate((1, 2, 4, 6)):
         tok_copy(t, dz, flip(t, k)).start()
@@ -173,7 +182,8 @@
     for c in range(per):
         load_down[c].wait()
         for h in range(QUARTERS):
-            dcast[c, rows_of(h)] = d32[pl.ds(c * tall + h * quarter, quarter)].astype(BF16)
+            block = rows_of(h)
+            dcast[c, block] = d32[pl.ds(c * tall + block.start, block.size)].astype(BF16)
 
         @pl.when(t == f * per + c)
         def _():
@@ -266,11 +276,11 @@
 
     tile = 512
 
-    def accumulate(src, first):
+    def accumulate(src, first, parts=range(per)):
         def one(n, _):
             w, column = n // (wbuf.shape[3] // tile), pl.multiple_of(n % (wbuf.shape[3] // tile) * tile, tile)
             total = 0.0 if first else acc[w, :, pl.ds(column, tile)]
-            for p in range(per):
+            for p in parts:
                 total = total + jnp.dot(
                     tbuf[src * per + p],
                     wbuf[w, src, pl.ds(p * width, width), pl.ds(column, tile)],
@@ -319,6 +329,9 @@
         def _():
             for n in range(2, 6):
                 chain_next(n)
+            for k, to in ((4, fx), (5, fx), (2, fy), (3, fy)):
+                for h in DUAL:
+                    hand(k, h, to)
 
         for place, k, to in ((1, 2, fy), (2, 4, fx)):
             @pl.when(q == place)
@@ -334,19 +347,12 @@
             hand(6, 0, fx)
             hand(6, 1, fy)
 
-    with scope("fd_wait"):
-        for i in range(CHUNKS):
-            w_copy(fd, i, fx).wait_recv()
-    with scope("fd_dot"):
-        accumulate(fd, False)
-
-    with scope("late"):
-        @pl.when(q == 0)
-        def _():
-            for j in range(2):
-                for h in DUAL:
-                    hand(2 + j, h, fy)
-                    hand(4 + j, h, fx)
+    for p in range(per):
+        with scope("fd_wait"):
+            for i in (2 * p, 2 * p + 1):
+                w_copy(fd, i, fx).wait_recv()
+        with scope("fd_dot"):
+            accumulate(fd, False, (p,))
 
     def make_hidden(n, _):
         columns = pl.ds(pl.multiple_of(n * tile, tile), tile)
@@ -416,7 +422,8 @@
     def turn(i):
         k = i
         for here, order in (
-            (jnp.logical_and(inner, q == 2), (0, 1, 4, 2, 5, 6, 3, 7)),
+            (jnp.logical_and(inner, q == 1), (0, 1, 2, 3, 4, 6, 5, 7)),
+            (jnp.logical_and(inner, q == 2), (0, 1, 2, 4, 5, 6, 3, 7)),
             (jnp.logical_and(inner, q == 3), (0, 1, 2, 4, 6, 7, 3, 5)),
             (jnp.logical_and(jnp.logical_not(inner), q % 2 == 0), (0, 1, 6, 7, 4, 5, 2, 3)),
             (jnp.logical_and(jnp.logical_not(inner), q % 2 == 1), (0, 1, 6, 7, 4, 2, 5, 3)),
@@ -430,41 +437,38 @@
     def pass_on(i):
         @pl.when(jnp.logical_and(side, i == 2))
         def _():
-            chain_next(i)
-
-        @pl.when(jnp.logical_and(side, jnp.logical_and(i >= 2, i <= 4)))
-        def _():
-            chain_next(i + 1)
+            for n in range(2, 6):
+                chain_next(n)
 
         for place, k, to in ((1, 3, fy), (2, 5, fx)):
-            @pl.when(jnp.logical_and(q == place, i == 4))
+            @pl.when(jnp.logical_and(q == place, i == 2))
             def _():
                 for h in DUAL:
                     d_copy(flip(base, k), h, to).start()
 
         @pl.when(jnp.logical_and(q == 3, i == 2))
         def _():
-            chain_next(i - 2)
-            chain_next(i - 1)
+            chain_next(0)
+            chain_next(1)
             hand(7, 0, fx)
             hand(7, 1, fy)
 
         @pl.when(jnp.logical_and(q == 3, jnp.logical_and(i >= 3, i <= 4)))
         def _():
-            chain_next(i - 1)
-
-        @pl.when(jnp.logical_and(q == 3, jnp.logical_and(i >= 4, i <= 5)))
-        def _():
-            chain_next(i)
+            chain_next(2 * i - 4)
+            chain_next(2 * i - 3)
 
     def step(i, _):
         with scope("pass_on"):
             pass_on(i)
 
-        @pl.when(i >= 1)
+        last = i - 1 - jnp.where(jnp.logical_or(q == 0, i >= n_tp), 1, 0)
+        now = jnp.logical_or(q == 0, i != n_tp - 1)
+
+        @pl.when(jnp.logical_and(now, jnp.logical_and(last >= 0, last < n_tp)))
         def _():
             with scope("finish"):
-                finish(turn(i - 1))
+                finish(turn(last))
 
         @pl.when(i < n_tp)
         def _():
@@ -476,7 +480,7 @@
 
         return 0
 
-    lax.fori_loop(0, n_tp + 1, step, 0)
+    lax.fori_loop(0, n_tp + 2, step, 0)
 
     with scope("sent"):
         sent(tbuf.at[pl.ds(0, n_tp - 1)], tok_s)
@@ -487,18 +491,18 @@
         def _():
             sent(dcast.at[0], dz_s)
             sent(xbuf, zr_s)
-            sent(dbuf.at[pl.ds(0, 7)], d_s)
+            sent(dbuf.at[:, pl.ds(0, 3 * tall // 4 + short // 2)], d_s)
 
         @pl.when(side)
         def _():
             sent(xbuf.at[:, :, rows_of(0)], o_s)
             sent(xbuf.at[0, 0], zr_s)
-            sent(dbuf.at[pl.ds(0, 7), pl.ds(0, 2 * quarter)], d_s)
+            sent(dbuf.at[:, pl.ds(0, 3 * tall // 8 + short // 4)], d_s)
 
         @pl.when(q == 3)
         def _():
             sent(xbuf.at[0], o_s)
-            sent(dbuf.at[pl.ds(0, 6)], d_s)
+            sent(dbuf.at[:, pl.ds(0, tall // 2 + short)], d_s)
 
         @pl.when(q != 0)
         def _():
@@ -553,7 +557,7 @@
             pltpu.VMEM((2, rows, cols), F32),
             pltpu.VMEM(down_train.shape, F32),
             pltpu.VMEM((n_tp // n_fs, tall, width), BF16),
-            pltpu.VMEM((3, n_tp // n_fs, tall // QUARTERS * len(DUAL), width), BF16),
+            pltpu.VMEM((3, n_tp // n_fs, tall - tall * CHAIN_SHARE // 8, width), BF16),
             pltpu.VMEM((n_tp, n_tok, width), BF16),
             pltpu.VMEM((2, n_tok, cols), F32),
             pltpu.VMEM((n_tok, cols), BF16),

time: 132 us -> 129 us (0.977)
  Pallas kernels: 131 us -> 128 us
    pallas_call x1, Pallas kernels: 126 us -> 123 us  [body(): pl.pallas_call(kernel, out_shape=(pltpu.VMEM((2, n_fs, rows, cols), BF16)...]
where the time goes in v3:
time: 129 us; the launch traced here: 128 us
  Pallas kernels  128 us (99%)
    pallas_call x1, Pallas kernels, body(): pl.pallas_call(kernel, out_shape=(pltpu.VMEM((2, n_fs, rows, cols), BF16)...  123 us
    pallas_call x1, Pallas kernels, body(): pl.pallas_call(write_out, out_shape=(jax.ShapeDtypeStruct((rows * n_fs, c...  4.77 us

profile of v3, /device:TPU:0, one launch (start us, length us, event | category | flops | bytes accessed | tf_op | source)
XLA Modules:
  0.0 128.4 jit_solution(8436185393869414001)
XLA Ops:
  0.6 123.0 %shard_map.84 = (bf16[2,4,512,1024]{3,2,1,0:T(8,128)(2,1)S(1)}, bf16[8,1024,256]{2,1,0:T(8,128)(2,1)S(1)}, bf16[64,2048]{1,0:T(8,128)(2,1)S(1)}) custom-call(bf16[512,256]{1,0:T(8,128)(2,1)} %tok_in.1, f32[1,512]{1,0:T(1,128)} %bitcast.1, f32[512,1024]{1,0:T(8,128)} %gate_in.1, f32[512,1024]{1,0:T(8,128)} %up_in.1, f32[2048,256]{1,0:T(8,128)} %down_in.1), custom_call_target="tpu_custom_call" | custom-call | tf_op jit(solution)/shard_map/pallas_call | solution.py:546
  123.6 4.8 %shard_map.85 = (bf16[2048,1024]{1,0:T(8,128)(2,1)}, bf16[2048,1024]{1,0:T(8,128)(2,1)}, bf16[1024,2048]{1,0:T(8,128)(2,1)}, bf16[64,2048]{1,0:T(8,128)(2,1)}) custom-call(bf16[2,4,512,1024]{3,2,1,0:T(8,128)(2,1)S(1)} %get-tuple-element.7.weights, bf16[8,1024,256]{2,1,0:T(8,128)(2,1)S(1)} %get-tuple-element.8.down, bf16[64,2048]{1,0:T(8,128)(2,1)S(1)} %get-tuple-element.9.layer), custom_call_target="tpu_custom_call" | custom-call | tf_op jit(solution)/shard_map/pallas_call | solution.py:593

commit v4 on v3

--- a/solution.py
+++ b/solution.py
@@ -15,7 +15,7 @@
 X_ORDER = (0, 2, 1, 3)
 Y_ORDER = (1, 3, 0, 2)
 QUARTERS = 4
-CHAIN_SHARE = 2
+CHAIN_SHARE = 5
 DUAL = (0, 1)
 CHAIN = (2, 3)
 scope = jax.named_scope
@@ -45,7 +45,7 @@
     part = rows // CHUNKS
     w_ins = (gate_in, up_in)
     tall, width = dbuf.shape[1], dbuf.shape[2]
-    short = tall * CHAIN_SHARE // 16
+    short = tall * CHAIN_SHARE // 32
     long = tall // 2 - short
     per = n_tp // n_fs
     n_tok = tbuf.shape[1]
@@ -377,7 +377,8 @@
             zsend[k, b] = (keep[k, b] + precv[k, b].astype(F32)).astype(BF16)
         piece = flip(base, k)
         zrecv[z, piece] = zsend[k, z]
-        for dz in range(1, n_z):
+        far = jnp.where(inner, 2, 3)
+        for dz in (far, 5 - far, 1):
             z_copy(k, dz, piece).start()
 
     def product(k):
@@ -557,7 +558,7 @@
             pltpu.VMEM((2, rows, cols), F32),
             pltpu.VMEM(down_train.shape, F32),
             pltpu.VMEM((n_tp // n_fs, tall, width), BF16),
-            pltpu.VMEM((3, n_tp // n_fs, tall - tall * CHAIN_SHARE // 8, width), BF16),
+            pltpu.VMEM((3, n_tp // n_fs, tall - tall * CHAIN_SHARE // 16, width), BF16),
             pltpu.VMEM((n_tp, n_tok, width), BF16),
             pltpu.VMEM((2, n_tok, cols), F32),
             pltpu.VMEM((n_tok, cols), BF16),

time: 129 us -> 129 us (level)
  no operation moved by 1% of the time
where the time goes in v4:
time: 129 us
  Pallas kernels  128 us (99%)
    pallas_call x1, Pallas kernels, body(): pl.pallas_call(kernel, out_shape=(pltpu.VMEM((2, n_fs, rows, cols), BF16)...  123 us
    pallas_call x1, Pallas kernels, body(): pl.pallas_call(write_out, out_shape=(jax.ShapeDtypeStruct((rows * n_fs, c...  4.77 us

profile of v4, /device:TPU:0, one launch (start us, length us, event | category | flops | bytes accessed | tf_op | source)
XLA Modules:
  0.0 128.5 jit_solution(13569673408695415943)
XLA Ops:
  0.6 123.1 %shard_map.84 = (bf16[2,4,512,1024]{3,2,1,0:T(8,128)(2,1)S(1)}, bf16[8,1024,256]{2,1,0:T(8,128)(2,1)S(1)}, bf16[64,2048]{1,0:T(8,128)(2,1)S(1)}) custom-call(bf16[512,256]{1,0:T(8,128)(2,1)} %tok_in.1, f32[1,512]{1,0:T(1,128)} %bitcast.1, f32[512,1024]{1,0:T(8,128)} %gate_in.1, f32[512,1024]{1,0:T(8,128)} %up_in.1, f32[2048,256]{1,0:T(8,128)} %down_in.1), custom_call_target="tpu_custom_call" | custom-call | tf_op jit(solution)/shard_map/pallas_call | solution.py:547
  123.7 4.8 %shard_map.85 = (bf16[2048,1024]{1,0:T(8,128)(2,1)}, bf16[2048,1024]{1,0:T(8,128)(2,1)}, bf16[1024,2048]{1,0:T(8,128)(2,1)}, bf16[64,2048]{1,0:T(8,128)(2,1)}) custom-call(bf16[2,4,512,1024]{3,2,1,0:T(8,128)(2,1)S(1)} %get-tuple-element.7.weights, bf16[8,1024,256]{2,1,0:T(8,128)(2,1)S(1)} %get-tuple-element.8.down, bf16[64,2048]{1,0:T(8,128)(2,1)S(1)} %get-tuple-element.9.layer), custom_call_target="tpu_custom_call" | custom-call | tf_op jit(solution)/shard_map/pallas_call | solution.py:594

commit v5 on v4

--- a/solution.py
+++ b/solution.py
@@ -351,14 +351,22 @@
         with scope("fd_wait"):
             for i in (2 * p, 2 * p + 1):
                 w_copy(fd, i, fx).wait_recv()
-        with scope("fd_dot"):
-            accumulate(fd, False, (p,))
+        if p < per - 1:
+            with scope("fd_dot"):
+                accumulate(fd, False, (p,))
 
     def make_hidden(n, _):
         columns = pl.ds(pl.multiple_of(n * tile, tile), tile)
         s = scale[...]
-        g = acc[0, :, columns] * s
-        hidden[:, columns] = (g / (1.0 + jnp.exp(-g)) * (acc[1, :, columns] * s)).astype(BF16)
+        g, u = [
+            (acc[w, :, columns] + jnp.dot(
+                tbuf[fd * per + per - 1],
+                wbuf[w, fd, pl.ds((per - 1) * width, width), columns],
+                preferred_element_type=F32,
+            )) * s
+            for w in range(2)
+        ]
+        hidden[:, columns] = (g / (1.0 + jnp.exp(-g)) * u).astype(BF16)
         return 0
 
     with scope("hidden"):

time: 129 us -> 129 us (level)
  no operation moved by 1% of the time
where the time goes in v5:
time: 129 us; the launch traced here: 128 us
  Pallas kernels  128 us (99%)
    pallas_call x1, Pallas kernels, body(): pl.pallas_call(kernel, out_shape=(pltpu.VMEM((2, n_fs, rows, cols), BF16)...  123 us
    pallas_call x1, Pallas kernels, body(): pl.pallas_call(write_out, out_shape=(jax.ShapeDtypeStruct((rows * n_fs, c...  4.77 us

profile of v5, /device:TPU:0, one launch (start us, length us, event | category | flops | bytes accessed | tf_op | source)
XLA Modules:
  0.0 128.4 jit_solution(12975856039383224833)
XLA Ops:
  0.6 123.0 %shard_map.84 = (bf16[2,4,512,1024]{3,2,1,0:T(8,128)(2,1)S(1)}, bf16[8,1024,256]{2,1,0:T(8,128)(2,1)S(1)}, bf16[64,2048]{1,0:T(8,128)(2,1)S(1)}) custom-call(bf16[512,256]{1,0:T(8,128)(2,1)} %tok_in.1, f32[1,512]{1,0:T(1,128)} %bitcast.1, f32[512,1024]{1,0:T(8,128)} %gate_in.1, f32[512,1024]{1,0:T(8,128)} %up_in.1, f32[2048,256]{1,0:T(8,128)} %down_in.1), custom_call_target="tpu_custom_call" | custom-call | tf_op jit(solution)/shard_map/pallas_call | solution.py:555
  123.7 4.8 %shard_map.85 = (bf16[2048,1024]{1,0:T(8,128)(2,1)}, bf16[2048,1024]{1,0:T(8,128)(2,1)}, bf16[1024,2048]{1,0:T(8,128)(2,1)}, bf16[64,2048]{1,0:T(8,128)(2,1)}) custom-call(bf16[2,4,512,1024]{3,2,1,0:T(8,128)(2,1)S(1)} %get-tuple-element.7.weights, bf16[8,1024,256]{2,1,0:T(8,128)(2,1)S(1)} %get-tuple-element.8.down, bf16[64,2048]{1,0:T(8,128)(2,1)S(1)} %get-tuple-element.9.layer), custom_call_target="tpu_custom_call" | custom-call | tf_op jit(solution)/shard_map/pallas_call | solution.py:602
